TPU v7x, 512 devices: a whole 4x4x16 slice. The times are simulated.
512 devices in a mesh: ep: 128 (over z, x, core), tp: 4 (over y).
Axes of the slice: x: 4, y: 4, z: 16, core: 2. Of those that a mesh axis runs over, the one named last changes fastest.
Arguments:
- tokens: bfloat16 [512, 2048], P('ep', 'tp'), may hold values from -6 to 6
- norm_gain: bfloat16 [2048], P('tp'), may hold values from 0.099609375 to 1.8984375
- w_query: bfloat16 [2048, 2048], P('tp', 'ep'), may hold values from -0.125 to 0.125
- w_forget: bfloat16 [2048, 2048], P('tp', 'ep'), may hold values from -0.125 to 0.125
- w_input: bfloat16 [2048, 2048], P('tp', 'ep'), may hold values from -0.125 to 0.125
- forget_floor: float32 [2048], P('tp'), may hold values from 0 to 0.9
- head_gain: bfloat16 [128], replicated, may hold values from 0.099609375 to 1.8984375
- w_output: bfloat16 [2048, 2048], P('tp', 'ep'), may hold values from -0.125 to 0.125
- state: float32 [512, 16, 128, 128], P('ep', 'tp'), may hold values from -6 to 6
- ffn_gain: bfloat16 [2048], P('tp'), may hold values from 0.099609375 to 1.8984375
- route_experts: int32 [512, 2], P('ep'), may hold values from 0 to 7, all different within a row; in each aligned block of 4 rows (0 to 3, 4 to 7, ...) at most 2 rows name the same one
- route_weights: float32 [512, 2], P('ep'), may hold values from 0.1 to 1
- w_gate: bfloat16 [128, 2048, 448], P('ep', None, 'tp'), may hold values from -0.125 to 0.125
- w_up: bfloat16 [128, 2048, 448], P('ep', None, 'tp'), may hold values from -0.125 to 0.125
- w_down: bfloat16 [128, 448, 2048], P('ep', 'tp'), may hold values from -0.0625 to 0.0625
Outputs:
- mixed: bfloat16 [512, 2048], P('ep', 'tp')
- new_state: float32 [512, 16, 128, 128], P('ep', 'tp')
Inputs may be any that keep to these rules, and one draw needn't show every extreme that they name: `route_experts`: each row names two different experts. Among the rows of one index of ep, no expert is named by more than 2 rows, and in every draw some expert is named by exactly 2 of them.
All inputs are finite; a program needn't handle non-finite values.
Results may differ from a plain program's by a relative error of at most 0.014.
Values may be sent and summed in bfloat16 or wider, within the bound.
No kernel may reach another device: no remote copies, remote signals or barrier semaphores. Data moves between devices by JAX's collectives and lax.ppermute only.
A program may use at most 64 MiB of HBM per device.

v0:
```python
import jax
import jax.numpy as jnp
from jax import lax
from jax.sharding import Mesh
from jax.sharding import PartitionSpec as P

EXPERTS = 8
EP = ("ep_0", "ep_1", "ep_2")
EPS = 1e-06


def laid_out(blocks, dim):
    blocks = jnp.moveaxis(blocks, 0, dim)
    dims = blocks.shape
    return blocks.reshape(*dims[:dim], dims[dim] * dims[dim + 1], *dims[dim + 2 :])


def all_blocks(shard, axes, sequence):
    blocks = shard
    for k in sequence:
        blocks = lax.all_gather(blocks, axes[k])
    done = sequence[::-1]
    back = [done.index(k) for k in range(len(axes))]
    blocks = blocks.transpose(*back, *range(len(axes), blocks.ndim))
    return blocks.reshape(-1, *shard.shape)


def whole_of(shard, axes, sequence, dim):
    return laid_out(all_blocks(shard, axes, sequence), dim)


def in_blocks(shard, dim, length):
    before, after = (shard.shape[:dim], shard.shape[dim + 1 :])
    return jnp.moveaxis(shard.reshape(*before, length, -1, *after), dim, 0)


def sent_and_summed(shard, axis, dim):
    length = lax.axis_size(axis)
    blocks = lax.all_to_all(in_blocks(shard, dim, length), axis, 0, 0, tiled=True)
    return jnp.sum(blocks, axis=0)


def summed_on_arrival(shard, axis, dim):
    blocks = in_blocks(shard, dim, lax.axis_size(axis))
    arrived = lax.all_to_all(blocks, axis, split_axis=0, concat_axis=0, tiled=True)
    return arrived.astype(jnp.float32).sum(axis=0)


def shards(
    tokens,
    norm_gain,
    w_query,
    w_forget,
    w_input,
    forget_floor,
    head_gain,
    w_output,
    state,
    ffn_gain,
    route_experts,
    route_weights,
    w_gate,
    w_up,
    w_down,
):
    ep_count = lax.axis_size(EP)
    tp_count = lax.axis_size("tp")
    seq_count = tokens.shape[0]
    model_width = tokens.shape[1] * tp_count
    head_size = state.shape[2]
    local_heads = state.shape[1]
    tok_f32 = tokens.astype(jnp.float32)
    sum_sq = lax.psum(jnp.sum(tok_f32 * tok_f32, axis=1), "tp")
    normed = (
        tok_f32 * lax.rsqrt(sum_sq / model_width + EPS)[:, None] * norm_gain.astype(jnp.float32)
    ).astype(jnp.bfloat16)
    w_joint = jnp.concatenate([w_query, w_forget, w_input], axis=1)
    partial_value = jnp.dot(
        whole_of(normed, EP, (1, 0, 2), 0), w_joint, preferred_element_type=jnp.float32
    )
    moved_in = lax.all_to_all(partial_value, EP, split_axis=0, concat_axis=1, tiled=True)
    summed = sent_and_summed(moved_in, "tp", 1)
    col_count = w_query.shape[1]
    blocks = summed.reshape(seq_count, -1, 3, col_count)
    queries = blocks[:, :, 0, :].reshape(seq_count, local_heads, head_size)
    fgate = blocks[:, :, 1, :].reshape(seq_count, local_heads, head_size)
    inputs = blocks[:, :, 2, :].reshape(seq_count, local_heads, head_size)
    floors = forget_floor.reshape(local_heads, head_size)
    forget = floors + (1.0 - floors) * jax.nn.sigmoid(fgate)
    new_state = forget[..., None] * state + (1.0 - forget)[..., None] * inputs[:, :, None, :]
    reads = jnp.einsum(
        "bhk,bhkv->bhv", jax.nn.silu(queries), new_state, precision=lax.Precision.HIGHEST
    )
    head_sq = jnp.mean(reads * reads, axis=-1, keepdims=True)
    heads_out = (
        (reads * lax.rsqrt(head_sq + EPS) * head_gain.astype(jnp.float32))
        .reshape(seq_count, local_heads * head_size)
        .astype(jnp.bfloat16)
    )
    part_out = jnp.dot(
        whole_of(heads_out, EP, (1, 0, 2), 0), w_output, preferred_element_type=jnp.float32
    )
    moved_out = lax.all_to_all(
        part_out.astype(jnp.bfloat16), EP, split_axis=0, concat_axis=1, tiled=True
    ).astype(part_out.dtype)
    mixer_slice = summed_on_arrival(moved_out.astype(jnp.bfloat16), "tp", 1).astype(jnp.bfloat16)
    middle = (tok_f32 + mixer_slice.astype(jnp.float32)).astype(jnp.bfloat16)
    middle_f32 = middle.astype(jnp.float32)
    span_count = ep_count // EXPERTS
    capacity = max(2, seq_count // 2)
    positions = jnp.arange(seq_count, dtype=jnp.int32)
    earlier = positions[None, :] < positions[:, None]
    same_expert = route_experts[:, :, None, None] == route_experts[None, None, :, :]
    slot_rank = jnp.sum(same_expert & earlier[:, None, :, None], axis=(2, 3))
    owners = jnp.arange(ep_count, dtype=jnp.int32) // span_count
    matched = route_experts[None, :, :] == owners[:, None, None]
    placed = slot_rank[:, :, None] == jnp.arange(capacity, dtype=jnp.int32)[None, None, :]
    slot_hits = matched[:, :, :, None] & placed[None, :, :, :]
    chosen = jnp.sum(slot_hits.astype(jnp.float32), axis=2).astype(jnp.bfloat16)
    weight_hits = jnp.sum(slot_hits.astype(jnp.float32) * route_weights[None, :, :, None], axis=2)
    row_stat = lax.psum(jnp.sum(middle_f32 * middle_f32, axis=1), "tp")
    second = (
        middle_f32 * lax.rsqrt(row_stat / model_width + EPS)[:, None] * ffn_gain.astype(jnp.float32)
    ).astype(jnp.bfloat16)
    outgoing = jnp.einsum("pts,td->psd", chosen, second, preferred_element_type=jnp.float32).astype(
        jnp.bfloat16
    )
    arrived_part = lax.all_to_all(outgoing, EP, split_axis=0, concat_axis=0, tiled=True)
    arrived = lax.all_gather(arrived_part, "tp", axis=2, tiled=True)
    expert_rows = arrived.reshape(ep_count * capacity, model_width)
    gate_act = jnp.dot(expert_rows, w_gate[0], preferred_element_type=jnp.float32)
    up_act = jnp.dot(expert_rows, w_up[0], preferred_element_type=jnp.float32)
    hidden = (jax.nn.silu(gate_act) * up_act).astype(jnp.bfloat16)
    piece_out = jnp.dot(hidden, w_down[0], preferred_element_type=jnp.float32)
    piece_total = summed_on_arrival(piece_out.astype(jnp.bfloat16), "tp", 1)
    returned = lax.all_to_all(
        piece_total.reshape(ep_count, capacity, -1).astype(jnp.bfloat16),
        EP,
        split_axis=0,
        concat_axis=0,
        tiled=True,
    ).astype(jnp.float32)
    routed = jnp.einsum("pts,psd->td", weight_hits, returned, precision=lax.Precision.HIGHEST)
    result = (middle_f32 + routed).astype(jnp.bfloat16)
    return (result, new_state)


def solution(mesh):
    torus = Mesh(mesh.devices.reshape(16, 4, 2, mesh.shape["tp"]), ("ep_0", "ep_1", "ep_2", "tp"))
    in_specs = (
        P(EP, "tp"),
        P("tp"),
        P("tp", EP),
        P("tp", EP),
        P("tp", EP),
        P("tp"),
        P(),
        P("tp", EP),
        P(EP, "tp", None, None),
        P("tp"),
        P(EP, None),
        P(EP, None),
        P(EP, None, "tp"),
        P(EP, None, "tp"),
        P(EP, "tp", None),
    )
    out_specs = (P(EP, "tp"), P(EP, "tp", None, None))
    return jax.shard_map(
        shards, mesh=torus, in_specs=in_specs, out_specs=out_specs, check_vma=False
    )
```

profile of v0, /device:TPU:33, one launch (start us, length us, event | category | flops | bytes accessed | tf_op | source)
XLA Modules:
  0.0 324.9 jit_solution(1485527307813868062)
XLA Ops:
  7.2 0.9 fusion.22
  8.0 8.7 %psum.14 = f32[4]{0:T(128)S(1)} all-reduce(f32[4]{0:T(128)S(1)} %fusion.22), channel_id=1, replica_groups=mesh['ep_0'=16,'ep_1'=4,'ep_2'=2,'tp'=4] {'tp'}, use_global_device_ids=true, to_apply=%region_1.0 | all-reduce | flops 4 | bytes 32 | tf_op jit(solution)/shard_map/psum | solution.py:73
  16.8 0.7 convert_element_type.76
  17.5 0.8 fusion.31
  18.2 9.5 %all-gather.5 = bf16[4,4,512]{2,1,0:T(4,128)(2,1)S(1)} all-gather(bf16[1,4,512]{2,1,0:T(4,128)(2,1)S(1)} %fusion.31), channel_id=2, replica_groups=mesh['ep_0'=16,'ep_1'=4,'ep_2'=2,'tp'=4] {'ep_1'}, dimensions={0}, use_global_device_ids=true | all-gather | bytes 20480 | tf_op jit(solution)/shard_map/all_gather | solution.py:21
  27.7 27.8 %all-gather.1 = bf16[64,4,512]{2,1,0:T(4,128)(2,1)S(1)} all-gather(bf16[4,4,512]{2,1,0:T(4,128)(2,1)S(1)} %all-gather.5), channel_id=3, replica_groups=mesh['ep_0'=16,'ep_1'=4,'ep_2'=2,'tp'=4] {'ep_0'}, dimensions={0}, use_global_device_ids=true | all-gather | bytes 278528 | tf_op jit(solution)/shard_map/all_gather | solution.py:21
  55.4 14.3 %all-gather.2 = bf16[32,4,4,512]{3,2,1,0:T(4,128)(2,1)S(1)} all-gather(bf16[16,4,4,512]{3,2,1,0:T(4,128)(2,1)S(1)} %bitcast.70), channel_id=4, replica_groups=mesh['ep_0'=16,'ep_1'=4,'ep_2'=2,'tp'=4] {'ep_2'}, dimensions={0}, use_global_device_ids=true | all-gather | bytes 786432 | tf_op jit(solution)/shard_map/all_gather | solution.py:21
  69.7 0.3 copy.120
  70.0 0.5 copy.121
  70.6 0.2 dot_general.26
  70.9 0.2 fusion.15
  71.1 0.2 copy.122
  71.3 1.0 reshape.148
  72.2 12.0 %all-to-all-start = ((f32[128,1,192]{2,1,0:T(1,128)}), f32[128,1,192]{2,1,0:T(1,128)S(1)}, u32[]{:S(2)}, u32[]{:S(2)}) async-start(f32[128,1,192]{2,1,0:T(1,128)} %reshape.148), calls=%async_computation | async-start | bytes 262144 | tf_op jit(solution)/shard_map/all_to_all | solution.py:81
  84.4 17.0 %all-to-all-done = f32[128,1,192]{2,1,0:T(1,128)S(1)} async-done(((f32[128,1,192]{2,1,0:T(1,128)}), f32[128,1,192]{2,1,0:T(1,128)S(1)}, u32[]{:S(2)}, u32[]{:S(2)}) %all-to-all-start) | async-done | bytes 98336 | tf_op jit(solution)/shard_map/all_to_all | solution.py:81
  101.4 0.5 broadcast.148
  101.9 1.0 reduce.10
  102.8 0.2 reshape.149
  103.1 0.2 reshape.118
  103.3 0.7 copy.124
  103.9 3.3 %all-to-all-start.1 = ((f32[4,4,1536]{2,1,0:T(4,128)}), f32[4,4,1536]{2,1,0:T(4,128)S(1)}, u32[]{:S(2)}, u32[]{:S(2)}) async-start(f32[4,4,1536]{2,1,0:T(4,128)} %copy.124), calls=%async_computation.1 | async-start | bytes 196608 | tf_op jit(solution)/shard_map/all_to_all | solution.py:39
  107.2 0.2 convert_reduce_fusion
  107.5 4.4 %all-to-all-done.1 = f32[4,4,1536]{2,1,0:T(4,128)S(1)} async-done(((f32[4,4,1536]{2,1,0:T(4,128)}), f32[4,4,1536]{2,1,0:T(4,128)S(1)}, u32[]{:S(2)}, u32[]{:S(2)}) %all-to-all-start.1) | async-done | bytes 98336 | tf_op jit(solution)/shard_map/all_to_all | solution.py:39
  111.9 0.2 reshape.119
  112.1 0.4 slice_reduce_fusion
  112.5 0.1 mul.125
  112.6 0.1 reshape_squeeze.4
  112.9 0.1 div.41
  113.0 0.6 multiply_add_fusion
  113.6 1.0 copy-done.1
  114.6 1.0 fusion.38
  115.6 0.1 multiply_reduce_fusion
  115.8 9.1 %all_gather.43 = bf16[4,4,512]{2,1,0:T(4,128)(2,1)S(1)} all-gather(bf16[1,4,512]{2,1,0:T(4,128)(2,1)S(1)} %convert_element_type.80), channel_id=1, replica_groups=mesh['ep_0'=16,'ep_1'=4,'ep_2'=2,'tp'=4] {'ep_1'}, dimensions={0}, use_global_device_ids=true | all-gather | bytes 20480 | tf_op jit(solution)/shard_map/all_gather | solution.py:21
  124.9 20.2 %all-gather.3 = bf16[64,4,512]{2,1,0:T(4,128)(2,1)S(1)} all-gather(bf16[4,4,512]{2,1,0:T(4,128)(2,1)S(1)} %all_gather.43), channel_id=5, replica_groups=mesh['ep_0'=16,'ep_1'=4,'ep_2'=2,'tp'=4] {'ep_0'}, dimensions={0}, use_global_device_ids=true | all-gather | bytes 278528 | tf_op jit(solution)/shard_map/all_gather | solution.py:21
  145.1 13.3 %all-gather.4 = bf16[32,4,4,512]{3,2,1,0:T(4,128)(2,1)S(1)} all-gather(bf16[16,4,4,512]{3,2,1,0:T(4,128)(2,1)S(1)} %bitcast.71), channel_id=6, replica_groups=mesh['ep_0'=16,'ep_1'=4,'ep_2'=2,'tp'=4] {'ep_2'}, dimensions={0}, use_global_device_ids=true | all-gather | bytes 786432 | tf_op jit(solution)/shard_map/all_gather | solution.py:21
  158.4 0.3 copy.127
  158.7 0.4 copy.128
  159.2 0.1 reshape_reshape.4
  159.3 0.1 copy-done.6
  159.4 0.2 convolution_convert_fusion.2
  159.7 0.8 copy.129
  160.4 9.0 %all-to-all-start.2 = ((bf16[128,4,16]{2,1,0:T(4,128)(2,1)}), bf16[128,4,16]{2,1,0:T(4,128)(2,1)S(1)}, u32[]{:S(2)}, u32[]{:S(2)}) async-start(bf16[128,4,16]{2,1,0:T(4,128)(2,1)} %bitcast.15), calls=%async_computation.2 | async-start | bytes 262144 | tf_op jit(solution)/shard_map/all_to_all | solution.py:103
  169.5 17.1 %all-to-all-done.2 = bf16[128,4,16]{2,1,0:T(4,128)(2,1)S(1)} async-done(((bf16[128,4,16]{2,1,0:T(4,128)(2,1)}), bf16[128,4,16]{2,1,0:T(4,128)(2,1)S(1)}, u32[]{:S(2)}, u32[]{:S(2)}) %all-to-all-start.2) | async-done | bytes 16416 | tf_op jit(solution)/shard_map/all_to_all | solution.py:103
  186.6 0.2 reshape.120
  186.7 0.6 copy.131
  187.3 3.2 all-to-all-start.3
  190.7 0.1 fusion.21
  190.7 4.0 %all-to-all-done.3 = bf16[4,4,512]{2,1,0:T(4,128)(2,1)S(1)} async-done(((bf16[4,4,512]{2,1,0:T(4,128)(2,1)}), bf16[4,4,512]{2,1,0:T(4,128)(2,1)S(1)}, u32[]{:S(2)}, u32[]{:S(2)}) %all-to-all-start.3) | async-done | bytes 16416 | tf_op jit(solution)/shard_map/all_to_all | solution.py:45
  194.8 0.1 fusion.26
  194.9 6.9 %psum.15 = f32[4]{0:T(128)S(1)} all-reduce(f32[4]{0:T(128)S(1)} %fusion.26), channel_id=1, replica_groups=mesh['ep_0'=16,'ep_1'=4,'ep_2'=2,'tp'=4] {'tp'}, use_global_device_ids=true, to_apply=%region_9.10 | all-reduce | flops 4 | bytes 32 | tf_op jit(solution)/shard_map/psum | solution.py:121
  201.8 0.3 convolution_convert_fusion.1
  202.1 0.3 copy.132
  202.4 31.9 %all_to_all.54 = bf16[128,2,512]{2,1,0:T(2,128)(2,1)} all-to-all(bf16[128,2,512]{2,1,0:T(2,128)(2,1)S(1)} %copy.132), channel_id=1, replica_groups=mesh['ep_0'=16,'ep_1'=4,'ep_2'=2,'tp'=4] {'ep_0','ep_1','ep_2'}, dimensions={0} | all-to-all | bytes 524288 | tf_op jit(solution)/shard_map/all_to_all | solution.py:128
  234.4 20.6 %all-gather.8.cloned.1.call-done = bf16[128,2,2048]{2,1,0:T(2,128)(2,1)} async-done(((bf16[128,2,512]{2,1,0:T(2,128)(2,1)}), bf16[128,2,2048]{2,1,0:T(2,128)(2,1)}) %all-gather.8.cloned.1.call-update) | async-done | bytes 1048592 | tf_op jit(solution)/shard_map/all_gather | solution.py:129
  255.0 1.5 reshape.121
  256.5 0.5 fusion.6
  257.0 0.5 copy-done.3
  257.5 1.4 convolution_convert_fusion
  258.9 0.1 copy.142
  259.0 16.2 %all_to_all.55 = bf16[4,256,512]{2,1,0:T(8,128)(2,1)S(1)} all-to-all(bf16[4,256,512]{2,1,0:T(8,128)(2,1)S(1)} %bitcast.67), channel_id=1, replica_groups=mesh['ep_0'=16,'ep_1'=4,'ep_2'=2,'tp'=4] {'tp'}, dimensions={0} | all-to-all | bytes 2097152 | tf_op jit(solution)/shard_map/all_to_all | solution.py:45
  275.2 0.2 reduce_sum.95
  275.4 0.1 convert_element_type.93
  275.5 41.7 %all_to_all.56 = bf16[128,2,512]{2,1,0:T(2,128)(2,1)S(1)} all-to-all(bf16[128,2,512]{2,1,0:T(2,128)(2,1)S(1)} %convert_element_type.93), channel_id=1, replica_groups=mesh['ep_0'=16,'ep_1'=4,'ep_2'=2,'tp'=4] {'ep_0','ep_1','ep_2'}, dimensions={0} | all-to-all | bytes 524288 | tf_op jit(solution)/shard_map/all_to_all | solution.py:136
  317.2 0.8 fusion.2
  (50 shorter events, 0.6 us)
Async XLA Ops:
  7.2 249.8 %copy-start = (bf16[1,112,2048]{2,1,0:T(8,128)(2,1)S(1)}, bf16[1,112,2048]{2,1,0:T(8,128)(2,1)}, u32[]{:S(2)}) copy-start(bf16[1,112,2048]{2,1,0:T(8,128)(2,1)} %param.29) | copy-start | bytes 1376260
  70.0 0.8 copy-start.7
  70.0 0.8 copy-start.8
  70.0 0.8 copy-start.9
  70.8 13.4 %copy-start.10 = (s32[4,2]{0,1:T(2,128)S(1)}, s32[4,2]{0,1:T(2,128)}, u32[]{:S(2)}) copy-start(s32[4,2]{0,1:T(2,128)} %param.25) | copy-start | bytes 100
  70.8 13.5 %copy-start.14 = (bf16[128]{0:T(256)(128)(2,1)S(1)}, bf16[128]{0:T(256)(128)(2,1)}, u32[]{:S(2)}) copy-start(bf16[128]{0:T(256)(128)(2,1)} %param.21) | copy-start | bytes 772
  70.9 13.5 %copy-start.11 = (f32[512]{0:T(512)S(1)}, f32[512]{0:T(512)}, u32[]{:S(2)}) copy-start(f32[512]{0:T(512)} %param.20) | copy-start | bytes 6148
  72.2 29.1 %all-to-all-start = ((f32[128,1,192]{2,1,0:T(1,128)}), f32[128,1,192]{2,1,0:T(1,128)S(1)}, u32[]{:S(2)}, u32[]{:S(2)}) async-start(f32[128,1,192]{2,1,0:T(1,128)} %reshape.148), calls=%async_computation | async-start | bytes 262144 | tf_op jit(solution)/shard_map/all_to_all | solution.py:81
  103.0 10.0 %copy-start.2 = (f32[4,4,128,128]{3,2,1,0:T(8,128)S(1)}, f32[4,4,128,128]{3,2,1,0:T(8,128)}, u32[]{:S(2)}) copy-start(f32[4,4,128,128]{3,2,1,0:T(8,128)} %param.23) | copy-start | bytes 3145732
  103.9 7.9 %all-to-all-start.1 = ((f32[4,4,1536]{2,1,0:T(4,128)}), f32[4,4,1536]{2,1,0:T(4,128)S(1)}, u32[]{:S(2)}, u32[]{:S(2)}) async-start(f32[4,4,1536]{2,1,0:T(4,128)} %copy.124), calls=%async_computation.1 | async-start | bytes 196608 | tf_op jit(solution)/shard_map/all_to_all | solution.py:39
  113.6 1.0 copy-start.1
  158.7 0.7 copy-start.6
  159.1 31.5 %copy-start.12 = (f32[4,2]{0,1:T(2,128)S(1)}, f32[4,2]{0,1:T(2,128)}, u32[]{:S(2)}) copy-start(f32[4,2]{0,1:T(2,128)} %param.26) | copy-start | bytes 100
  159.1 35.6 %copy-start.5 = (bf16[4,512]{1,0:T(4,128)(2,1)S(1)}, bf16[4,512]{1,0:T(4,128)(2,1)}, u32[]{:S(2)}) copy-start(bf16[4,512]{1,0:T(4,128)(2,1)} %param.15) | copy-start | bytes 12292
  159.2 35.8 %copy-start.13 = (bf16[512]{0:T(512)(128)(2,1)S(1)}, bf16[512]{0:T(512)(128)(2,1)}, u32[]{:S(2)}) copy-start(bf16[512]{0:T(512)(128)(2,1)} %param.24) | copy-start | bytes 3076
  160.4 26.1 %all-to-all-start.2 = ((bf16[128,4,16]{2,1,0:T(4,128)(2,1)}), bf16[128,4,16]{2,1,0:T(4,128)(2,1)S(1)}, u32[]{:S(2)}, u32[]{:S(2)}) async-start(bf16[128,4,16]{2,1,0:T(4,128)(2,1)} %bitcast.15), calls=%async_computation.2 | async-start | bytes 262144 | tf_op jit(solution)/shard_map/all_to_all | solution.py:103
  187.3 7.4 %all-to-all-start.3 = ((bf16[4,4,512]{2,1,0:T(4,128)(2,1)}), bf16[4,4,512]{2,1,0:T(4,128)(2,1)S(1)}, u32[]{:S(2)}, u32[]{:S(2)}) async-start(bf16[4,4,512]{2,1,0:T(4,128)(2,1)} %copy.131), calls=%async_computation.3 | async-start | bytes 32768 | tf_op jit(solution)/shard_map/all_to_all | solution.py:45
  190.6 64.4 %all-gather.8.cloned.1.call-start = ((), (), s32[]{:S(2)}) async-start(), calls=%async_computation.7 | async-start | bytes 1310720 | tf_op jit(solution)/shard_map/all_gather | solution.py:129
  234.4 22.1 %copy-start.4 = (bf16[1,2048,112]{1,2,0:T(8,128)(2,1)S(1)}, bf16[1,2048,112]{1,2,0:T(8,128)(2,1)}, u32[]{:S(2)}) copy-start(bf16[1,2048,112]{1,2,0:T(8,128)(2,1)} %param.27) | copy-start | bytes 1376260
  256.4 1.0 copy-start.3
Sparse Core Ops, SparseCore 0:
  234.5 20.4 all-gather.7
where the time goes:
time: 326 us; the launch traced here: 325 us
  blocking collectives  200 us (61%)
  waiting for transfers between devices  63.1 us (19%)
  starting transfers between devices  27.6 us (8%)
  between operations  14.5 us (4%)
  local copies, waits for them, and re-layouts  10.8 us (3%)
  other arithmetic  4.91 us (2%)
  matrix products  4.43 us (1%)
    all_gather x6, blocking collectives, all_blocks(): blocks = lax.all_gather(blocks, axes[k])  94.2 us
    all_to_all x1, blocking collectives, shards(): lax.all_to_all(piece_total.reshape(ep_count, capacity, -1).astype(jnp.bfl...  41.7 us
    all_to_all x1, blocking collectives, shards(): lax.all_to_all(outgoing, EP, split_axis=0, concat_axis=0, tiled=True)  31.9 us
    all_gather x1, waiting for transfers between devices, shards(): arrived = lax.all_gather(arrived_part, 'tp', axis=2, tiled=True)  20.6 us
    all_to_all x1, waiting for transfers between devices, shards(): lax.all_to_all(part_out.astype(jnp.bfloat16), EP, split_axis=0, concat_ax...  17.1 us
    all_to_all x1, waiting for transfers between devices, shards(): lax.all_to_all(partial_value, EP, split_axis=0, concat_axis=1, tiled=True)  17 us
    all_to_all x1, blocking collectives, summed_on_arrival(): lax.all_to_all(blocks, axis, split_axis=0, concat_axis=0, tiled=True)  16.2 us
    all_to_all x1, starting transfers between devices, shards(): lax.all_to_all(partial_value, EP, split_axis=0, concat_axis=1, tiled=True)  12 us
  transfers between devices with their start and end apart: 5, of which 5 were waited for; matrix products, arithmetic and copies ran while one was open for 0% of the time, Pallas kernels for 0%

commit v1 on v0

--- a/solution.py
+++ b/solution.py
@@ -7,6 +7,27 @@
 EXPERTS = 8
 EP = ("ep_0", "ep_1", "ep_2")
 EPS = 1e-06
+
+
+def ring_gather(shard, axis, dim):
+    peers, index, rows = (lax.axis_size(axis), lax.axis_index(axis), shard.shape[dim])
+    right = [(i, (i + 1) % peers) for i in range(peers)]
+    downward = [(i, (i - 1) % peers) for i in range(peers)]
+    out = jnp.zeros((*shard.shape[:dim], peers * rows, *shard.shape[dim + 1 :]), shard.dtype)
+    out = lax.dynamic_update_slice_in_dim(out, shard, index * rows, axis=dim)
+    from_left = from_right = shard
+    halfway = peers // 2
+    for step in range(1, halfway + 1):
+        from_left = lax.ppermute(from_left, axis, right)
+        out = lax.dynamic_update_slice_in_dim(
+            out, from_left, (index - step) % peers * rows, axis=dim
+        )
+        if step < peers - halfway:
+            from_right = lax.ppermute(from_right, axis, downward)
+            out = lax.dynamic_update_slice_in_dim(
+                out, from_right, (index + step) % peers * rows, axis=dim
+            )
+    return out
 
 
 def laid_out(blocks, dim):
@@ -126,7 +147,7 @@
         jnp.bfloat16
     )
     arrived_part = lax.all_to_all(outgoing, EP, split_axis=0, concat_axis=0, tiled=True)
-    arrived = lax.all_gather(arrived_part, "tp", axis=2, tiled=True)
+    arrived = ring_gather(arrived_part, "tp", 2)
     expert_rows = arrived.reshape(ep_count * capacity, model_width)
     gate_act = jnp.dot(expert_rows, w_gate[0], preferred_element_type=jnp.float32)
     up_act = jnp.dot(expert_rows, w_up[0], preferred_element_type=jnp.float32)

time: 326 us -> 301 us (0.923)
  between operations: 14.5 us -> 1.22 us
  blocking collectives: 200 us -> 188 us
  waiting for transfers between devices: 63.1 us -> 53.2 us
  starting transfers between devices: 27.6 us -> 36 us
    all_gather x1 -> x0, waiting for transfers between devices: 20.6 us -> none  [shards(): arrived = lax.all_gather(arrived_part, 'tp', axis=2, tiled=True)]
    ppermute x0 -> x3, waiting for transfers between devices: none -> 10.7 us  [the longest x2 10.7 us: ring_gather(): from_left = lax.ppermute(from_left, axis, right)]
    all_to_all x1, blocking collectives: 41.7 us -> 31.6 us  [shards(): lax.all_to_all(piece_total.reshape(ep_count, capacity, -1).astype(jnp.bfl...]
    ppermute x0 -> x3, starting transfers between devices: none -> 8.39 us  [the longest x2 4.38 us: ring_gather(): from_left = lax.ppermute(from_left, axis, right)]
  transfers between devices with their start and end apart: 5 -> 7, of which waited for: 5 -> 6; matrix products, arithmetic and copies ran while one was open for 0% -> 1% of each run, Pallas kernels for 0% -> 0%
where the time goes in v1:
time: 301 us; the launch traced here: 300 us
  blocking collectives  188 us (62%)
  waiting for transfers between devices  53.2 us (18%)
  starting transfers between devices  36 us (12%)
  local copies, waits for them, and re-layouts  10.7 us (4%)
  matrix products  5.52 us (2%)
  other arithmetic  4.91 us (2%)
    all_gather x6, blocking collectives, all_blocks(): blocks = lax.all_gather(blocks, axes[k])  94.2 us
    all_to_all x1, blocking collectives, shards(): lax.all_to_all(outgoing, EP, split_axis=0, concat_axis=0, tiled=True)  31.8 us
    all_to_all x1, blocking collectives, shards(): lax.all_to_all(piece_total.reshape(ep_count, capacity, -1).astype(jnp.bfl...  31.6 us
    all_to_all x1, waiting for transfers between devices, shards(): lax.all_to_all(part_out.astype(jnp.bfloat16), EP, split_axis=0, concat_ax...  17.1 us
    all_to_all x1, waiting for transfers between devices, shards(): lax.all_to_all(partial_value, EP, split_axis=0, concat_axis=1, tiled=True)  17 us
    all_to_all x1, blocking collectives, summed_on_arrival(): lax.all_to_all(blocks, axis, split_axis=0, concat_axis=0, tiled=True)  15.3 us
    all_to_all x1, starting transfers between devices, shards(): lax.all_to_all(partial_value, EP, split_axis=0, concat_axis=1, tiled=True)  12 us
    ppermute x2, waiting for transfers between devices, ring_gather(): from_left = lax.ppermute(from_left, axis, right)  10.7 us
  transfers between devices with their start and end apart: 7, of which 6 were waited for; matrix products, arithmetic and copies ran while one was open for 1% of the time, Pallas kernels for 0%

profile of v1, /device:TPU:33, one launch (start us, length us, event | category | flops | bytes accessed | tf_op | source)
XLA Modules:
  0.0 299.9 jit_solution(1138553459085530289)
XLA Ops:
  0.6 0.9 fusion.20
  1.5 0.7 convert_element_type.76
  2.2 8.7 %psum.14 = f32[4]{0:T(128)S(1)} all-reduce(f32[4]{0:T(128)S(1)} %fusion.20), channel_id=1, replica_groups=mesh['ep_0'=16,'ep_1'=4,'ep_2'=2,'tp'=4] {'tp'}, use_global_device_ids=true, to_apply=%region_1.0 | all-reduce | flops 4 | bytes 32 | tf_op jit(solution)/shard_map/psum | solution.py:94
  10.9 0.8 fusion.29
  11.7 9.5 %all-gather.5 = bf16[4,4,512]{2,1,0:T(4,128)(2,1)S(1)} all-gather(bf16[1,4,512]{2,1,0:T(4,128)(2,1)S(1)} %fusion.29), channel_id=2, replica_groups=mesh['ep_0'=16,'ep_1'=4,'ep_2'=2,'tp'=4] {'ep_1'}, dimensions={0}, use_global_device_ids=true | all-gather | bytes 20480 | tf_op jit(solution)/shard_map/all_gather | solution.py:42
  21.1 27.8 %all-gather.1 = bf16[64,4,512]{2,1,0:T(4,128)(2,1)S(1)} all-gather(bf16[4,4,512]{2,1,0:T(4,128)(2,1)S(1)} %all-gather.5), channel_id=3, replica_groups=mesh['ep_0'=16,'ep_1'=4,'ep_2'=2,'tp'=4] {'ep_0'}, dimensions={0}, use_global_device_ids=true | all-gather | bytes 278528 | tf_op jit(solution)/shard_map/all_gather | solution.py:42
  48.9 14.3 %all-gather.2 = bf16[32,4,4,512]{3,2,1,0:T(4,128)(2,1)S(1)} all-gather(bf16[16,4,4,512]{3,2,1,0:T(4,128)(2,1)S(1)} %bitcast.73), channel_id=4, replica_groups=mesh['ep_0'=16,'ep_1'=4,'ep_2'=2,'tp'=4] {'ep_2'}, dimensions={0}, use_global_device_ids=true | all-gather | bytes 786432 | tf_op jit(solution)/shard_map/all_gather | solution.py:42
  63.2 0.3 copy.129
  63.5 0.5 copy.130
  64.0 0.2 dot_general.26
  64.3 0.2 fusion.13
  64.6 0.2 copy.131
  64.7 1.0 reshape.148
  65.7 12.0 %all-to-all-start = ((f32[128,1,192]{2,1,0:T(1,128)}), f32[128,1,192]{2,1,0:T(1,128)S(1)}, u32[]{:S(2)}, u32[]{:S(2)}) async-start(f32[128,1,192]{2,1,0:T(1,128)} %reshape.148), calls=%async_computation | async-start | bytes 262144 | tf_op jit(solution)/shard_map/all_to_all | solution.py:102
  77.8 17.0 %all-to-all-done = f32[128,1,192]{2,1,0:T(1,128)S(1)} async-done(((f32[128,1,192]{2,1,0:T(1,128)}), f32[128,1,192]{2,1,0:T(1,128)S(1)}, u32[]{:S(2)}, u32[]{:S(2)}) %all-to-all-start) | async-done | bytes 98336 | tf_op jit(solution)/shard_map/all_to_all | solution.py:102
  94.8 0.5 broadcast.155
  95.3 1.0 reduce.10
  96.3 0.2 reshape.149
  96.5 0.2 reshape.118
  96.7 0.7 copy.133
  97.4 3.3 %all-to-all-start.1 = ((f32[4,4,1536]{2,1,0:T(4,128)}), f32[4,4,1536]{2,1,0:T(4,128)S(1)}, u32[]{:S(2)}, u32[]{:S(2)}) async-start(f32[4,4,1536]{2,1,0:T(4,128)} %copy.133), calls=%async_computation.1 | async-start | bytes 196608 | tf_op jit(solution)/shard_map/all_to_all | solution.py:60
  100.7 0.2 convert_reduce_fusion
  100.9 4.4 %all-to-all-done.1 = f32[4,4,1536]{2,1,0:T(4,128)S(1)} async-done(((f32[4,4,1536]{2,1,0:T(4,128)}), f32[4,4,1536]{2,1,0:T(4,128)S(1)}, u32[]{:S(2)}, u32[]{:S(2)}) %all-to-all-start.1) | async-done | bytes 98336 | tf_op jit(solution)/shard_map/all_to_all | solution.py:60
  105.3 0.2 reshape.119
  105.5 0.4 slice_reduce_fusion
  106.5 0.6 multiply_add_fusion
  107.1 1.0 copy-done.1
  108.0 1.0 fusion.36
  109.2 9.1 %all_gather.40 = bf16[4,4,512]{2,1,0:T(4,128)(2,1)S(1)} all-gather(bf16[1,4,512]{2,1,0:T(4,128)(2,1)S(1)} %convert_element_type.80), channel_id=1, replica_groups=mesh['ep_0'=16,'ep_1'=4,'ep_2'=2,'tp'=4] {'ep_1'}, dimensions={0}, use_global_device_ids=true | all-gather | bytes 20480 | tf_op jit(solution)/shard_map/all_gather | solution.py:42
  118.3 20.2 %all-gather.3 = bf16[64,4,512]{2,1,0:T(4,128)(2,1)S(1)} all-gather(bf16[4,4,512]{2,1,0:T(4,128)(2,1)S(1)} %all_gather.40), channel_id=5, replica_groups=mesh['ep_0'=16,'ep_1'=4,'ep_2'=2,'tp'=4] {'ep_0'}, dimensions={0}, use_global_device_ids=true | all-gather | bytes 278528 | tf_op jit(solution)/shard_map/all_gather | solution.py:42
  138.5 13.3 %all-gather.4 = bf16[32,4,4,512]{3,2,1,0:T(4,128)(2,1)S(1)} all-gather(bf16[16,4,4,512]{3,2,1,0:T(4,128)(2,1)S(1)} %bitcast.74), channel_id=6, replica_groups=mesh['ep_0'=16,'ep_1'=4,'ep_2'=2,'tp'=4] {'ep_2'}, dimensions={0}, use_global_device_ids=true | all-gather | bytes 786432 | tf_op jit(solution)/shard_map/all_gather | solution.py:42
  151.9 0.3 copy.136
  152.2 0.4 copy.137
  152.6 0.1 reshape_reshape.4
  152.7 0.1 copy-done.5
  152.9 0.2 convolution_convert_fusion.2
  153.1 0.8 copy.138
  153.9 9.0 %all-to-all-start.2 = ((bf16[128,4,16]{2,1,0:T(4,128)(2,1)}), bf16[128,4,16]{2,1,0:T(4,128)(2,1)S(1)}, u32[]{:S(2)}, u32[]{:S(2)}) async-start(bf16[128,4,16]{2,1,0:T(4,128)(2,1)} %bitcast.15), calls=%async_computation.2 | async-start | bytes 262144 | tf_op jit(solution)/shard_map/all_to_all | solution.py:124
  162.9 17.1 %all-to-all-done.2 = bf16[128,4,16]{2,1,0:T(4,128)(2,1)S(1)} async-done(((bf16[128,4,16]{2,1,0:T(4,128)(2,1)}), bf16[128,4,16]{2,1,0:T(4,128)(2,1)S(1)}, u32[]{:S(2)}, u32[]{:S(2)}) %all-to-all-start.2) | async-done | bytes 16416 | tf_op jit(solution)/shard_map/all_to_all | solution.py:124
  180.0 0.2 reshape.120
  180.2 0.6 copy.140
  180.8 3.2 %all-to-all-start.3 = ((bf16[4,4,512]{2,1,0:T(4,128)(2,1)}), bf16[4,4,512]{2,1,0:T(4,128)(2,1)S(1)}, u32[]{:S(2)}, u32[]{:S(2)}) async-start(bf16[4,4,512]{2,1,0:T(4,128)(2,1)} %copy.140), calls=%async_computation.3 | async-start | bytes 32768 | tf_op jit(solution)/shard_map/all_to_all | solution.py:66
  184.1 4.1 %all-to-all-done.3 = bf16[4,4,512]{2,1,0:T(4,128)(2,1)S(1)} async-done(((bf16[4,4,512]{2,1,0:T(4,128)(2,1)}), bf16[4,4,512]{2,1,0:T(4,128)(2,1)S(1)}, u32[]{:S(2)}, u32[]{:S(2)}) %all-to-all-start.3) | async-done | bytes 16416 | tf_op jit(solution)/shard_map/all_to_all | solution.py:66
  188.4 6.9 %psum.15 = f32[4]{0:T(128)S(1)} all-reduce(f32[4]{0:T(128)S(1)} %fusion.24), channel_id=1, replica_groups=mesh['ep_0'=16,'ep_1'=4,'ep_2'=2,'tp'=4] {'tp'}, use_global_device_ids=true, to_apply=%region_9.10 | all-reduce | flops 4 | bytes 32 | tf_op jit(solution)/shard_map/psum | solution.py:142
  195.3 0.3 convolution_convert_fusion.1
  195.6 0.3 copy.141
  195.8 31.8 %all_to_all.54 = bf16[128,2,512]{2,1,0:T(2,128)(2,1)S(1)} all-to-all(bf16[128,2,512]{2,1,0:T(2,128)(2,1)S(1)} %copy.141), channel_id=1, replica_groups=mesh['ep_0'=16,'ep_1'=4,'ep_2'=2,'tp'=4] {'ep_0','ep_1','ep_2'}, dimensions={0} | all-to-all | bytes 524288 | tf_op jit(solution)/shard_map/all_to_all | solution.py:149
  227.7 2.5 collective-permute-start
  230.1 4.0 %collective-permute-start.1 = (bf16[128,2,512]{2,1,0:T(2,128)(2,1)S(1)}, bf16[128,2,512]{2,1,0:T(2,128)(2,1)S(1)}, u32[]{:S(2)}, u32[]{:S(2)}) collective-permute-start(bf16[128,2,512]{2,1,0:T(2,128)(2,1)S(1)} %all_to_all.54), channel_id=1, source_target_pairs={{0,3},{1,0},{2,1},{3,2},{4,7},{5,4},{6,5},{7,6},{8,11},{9,8},{10,9... | collective-permute-start | bytes 786440 | tf_op jit(solution)/shard_map/ppermute | solution.py:26
  234.2 4.1 %collective-permute-done = bf16[128,2,512]{2,1,0:T(2,128)(2,1)S(1)} collective-permute-done((bf16[128,2,512]{2,1,0:T(2,128)(2,1)S(1)}, bf16[128,2,512]{2,1,0:T(2,128)(2,1)S(1)}, u32[]{:S(2)}, u32[]{:S(2)}) %collective-permute-start) | collective-permute-done | bytes 262176 | tf_op jit(solution)/shard_map/ppermute | solution.py:21
  238.3 1.9 collective-permute-start.2
  240.2 0.5 broadcast_in_dim.2
  240.8 0.2 constant_dynamic-update-slice_fusion.3
  241.0 0.2 constant_dynamic-update-slice_fusion.2
  241.3 0.2 constant_dynamic-update-slice_fusion.1
  241.5 6.6 %collective-permute-done.2 = bf16[128,2,512]{2,1,0:T(2,128)(2,1)S(1)} collective-permute-done((bf16[128,2,512]{2,1,0:T(2,128)(2,1)S(1)}, bf16[128,2,512]{2,1,0:T(2,128)(2,1)S(1)}, u32[]{:S(2)}, u32[]{:S(2)}) %collective-permute-start.2) | collective-permute-done | bytes 262176 | tf_op jit(solution)/shard_map/ppermute | solution.py:21
  248.1 0.2 constant_dynamic-update-slice_fusion
  248.3 0.4 reshape.121
  248.8 1.5 fusion.3
  250.4 1.4 convolution_convert_fusion
  251.9 15.3 %all_to_all.55 = bf16[4,256,512]{2,1,0:T(8,128)(2,1)S(1)} all-to-all(bf16[4,256,512]{2,1,0:T(8,128)(2,1)S(1)} %bitcast.70), channel_id=1, replica_groups=mesh['ep_0'=16,'ep_1'=4,'ep_2'=2,'tp'=4] {'tp'}, dimensions={0} | all-to-all | bytes 2097152 | tf_op jit(solution)/shard_map/all_to_all | solution.py:66
  267.2 0.2 reduce_sum.95
  267.5 31.6 %all_to_all.56 = bf16[128,2,512]{2,1,0:T(2,128)(2,1)S(1)} all-to-all(bf16[128,2,512]{2,1,0:T(2,128)(2,1)S(1)} %convert_element_type.93), channel_id=1, replica_groups=mesh['ep_0'=16,'ep_1'=4,'ep_2'=2,'tp'=4] {'ep_0','ep_1','ep_2'}, dimensions={0} | all-to-all | bytes 524288 | tf_op jit(solution)/shard_map/all_to_all | solution.py:157
  299.1 0.8 fusion.1
  (56 shorter events, 1.3 us)
Async XLA Ops:
  0.6 249.7 %copy-start = (bf16[1,112,2048]{2,1,0:T(8,128)(2,1)S(1)}, bf16[1,112,2048]{2,1,0:T(8,128)(2,1)}, u32[]{:S(2)}) copy-start(bf16[1,112,2048]{2,1,0:T(8,128)(2,1)} %param.29) | copy-start | bytes 1376260
  63.5 0.8 copy-start.6
  63.5 0.8 copy-start.7
  63.5 0.8 copy-start.8
  64.3 13.4 %copy-start.9 = (s32[4,2]{0,1:T(2,128)S(1)}, s32[4,2]{0,1:T(2,128)}, u32[]{:S(2)}) copy-start(s32[4,2]{0,1:T(2,128)} %param.25) | copy-start | bytes 100
  64.3 13.5 %copy-start.13 = (bf16[128]{0:T(256)(128)(2,1)S(1)}, bf16[128]{0:T(256)(128)(2,1)}, u32[]{:S(2)}) copy-start(bf16[128]{0:T(256)(128)(2,1)} %param.21) | copy-start | bytes 772
  64.3 13.5 %copy-start.10 = (f32[512]{0:T(512)S(1)}, f32[512]{0:T(512)}, u32[]{:S(2)}) copy-start(f32[512]{0:T(512)} %param.20) | copy-start | bytes 6148
  65.7 29.1 %all-to-all-start = ((f32[128,1,192]{2,1,0:T(1,128)}), f32[128,1,192]{2,1,0:T(1,128)S(1)}, u32[]{:S(2)}, u32[]{:S(2)}) async-start(f32[128,1,192]{2,1,0:T(1,128)} %reshape.148), calls=%async_computation | async-start | bytes 262144 | tf_op jit(solution)/shard_map/all_to_all | solution.py:102
  96.5 10.0 %copy-start.2 = (f32[4,4,128,128]{3,2,1,0:T(8,128)S(1)}, f32[4,4,128,128]{3,2,1,0:T(8,128)}, u32[]{:S(2)}) copy-start(f32[4,4,128,128]{3,2,1,0:T(8,128)} %param.23) | copy-start | bytes 3145732
  97.4 7.9 %all-to-all-start.1 = ((f32[4,4,1536]{2,1,0:T(4,128)}), f32[4,4,1536]{2,1,0:T(4,128)S(1)}, u32[]{:S(2)}, u32[]{:S(2)}) async-start(f32[4,4,1536]{2,1,0:T(4,128)} %copy.133), calls=%async_computation.1 | async-start | bytes 196608 | tf_op jit(solution)/shard_map/all_to_all | solution.py:60
  107.1 1.0 copy-start.1
  152.1 0.7 copy-start.5
  152.6 31.5 %copy-start.11 = (f32[4,2]{0,1:T(2,128)S(1)}, f32[4,2]{0,1:T(2,128)}, u32[]{:S(2)}) copy-start(f32[4,2]{0,1:T(2,128)} %param.26) | copy-start | bytes 100
  152.6 35.6 %copy-start.4 = (bf16[4,512]{1,0:T(4,128)(2,1)S(1)}, bf16[4,512]{1,0:T(4,128)(2,1)}, u32[]{:S(2)}) copy-start(bf16[4,512]{1,0:T(4,128)(2,1)} %param.15) | copy-start | bytes 12292
  152.6 35.8 %copy-start.12 = (bf16[512]{0:T(512)(128)(2,1)S(1)}, bf16[512]{0:T(512)(128)(2,1)}, u32[]{:S(2)}) copy-start(bf16[512]{0:T(512)(128)(2,1)} %param.24) | copy-start | bytes 3076
  153.9 26.1 %all-to-all-start.2 = ((bf16[128,4,16]{2,1,0:T(4,128)(2,1)}), bf16[128,4,16]{2,1,0:T(4,128)(2,1)S(1)}, u32[]{:S(2)}, u32[]{:S(2)}) async-start(bf16[128,4,16]{2,1,0:T(4,128)(2,1)} %bitcast.15), calls=%async_computation.2 | async-start | bytes 262144 | tf_op jit(solution)/shard_map/all_to_all | solution.py:124
  180.8 7.4 %all-to-all-start.3 = ((bf16[4,4,512]{2,1,0:T(4,128)(2,1)}), bf16[4,4,512]{2,1,0:T(4,128)(2,1)S(1)}, u32[]{:S(2)}, u32[]{:S(2)}) async-start(bf16[4,4,512]{2,1,0:T(4,128)(2,1)} %copy.140), calls=%async_computation.3 | async-start | bytes 32768 | tf_op jit(solution)/shard_map/all_to_all | solution.py:66
  227.7 10.6 %collective-permute-start = (bf16[128,2,512]{2,1,0:T(2,128)(2,1)S(1)}, bf16[128,2,512]{2,1,0:T(2,128)(2,1)S(1)}, u32[]{:S(2)}, u32[]{:S(2)}) collective-permute-start(bf16[128,2,512]{2,1,0:T(2,128)(2,1)S(1)} %all_to_all.54), channel_id=1, source_target_pairs={{0,1},{1,2},{2,3},{3,0},{4,5},{5,6},{6,7},{7,4},{8,9},{9,10},{10,1... | collective-permute-start | bytes 786440 | tf_op jit(solution)/shard_map/ppermute | solution.py:21
  230.1 11.1 %collective-permute-start.1 = (bf16[128,2,512]{2,1,0:T(2,128)(2,1)S(1)}, bf16[128,2,512]{2,1,0:T(2,128)(2,1)S(1)}, u32[]{:S(2)}, u32[]{:S(2)}) collective-permute-start(bf16[128,2,512]{2,1,0:T(2,128)(2,1)S(1)} %all_to_all.54), channel_id=1, source_target_pairs={{0,3},{1,0},{2,1},{3,2},{4,7},{5,4},{6,5},{7,6},{8,11},{9,8},{10,9... | collective-permute-start | bytes 786440 | tf_op jit(solution)/shard_map/ppermute | solution.py:26
  238.3 9.8 %collective-permute-start.2 = (bf16[128,2,512]{2,1,0:T(2,128)(2,1)S(1)}, bf16[128,2,512]{2,1,0:T(2,128)(2,1)S(1)}, u32[]{:S(2)}, u32[]{:S(2)}) collective-permute-start(bf16[128,2,512]{2,1,0:T(2,128)(2,1)S(1)} %collective-permute-done), channel_id=1, source_target_pairs={{0,1},{1,2},{2,3},{3,0},{4,5},{5,6},{6,7},{7,4},{8,9},{9,10},{10,1... | collective-permute-start | bytes 786440 | tf_op jit(solution)/shard_map/ppermute | solution.py:21
  248.8 1.6 copy-start.3
